TPU v7x, 256 devices: a whole 4x4x8 slice. The times are simulated.
256 devices in a mesh: ep: 64 (over z, y, core), tp: 4 (over x).
Axes of the slice: x: 4, y: 4, z: 8, core: 2. Of those that a mesh axis runs over, the one named last changes fastest.
Arguments:
- queries: bfloat16 [16384, 1536], P('ep', 'tp'), may hold values from -6 to 6
- kv_latent: bfloat16 [16384, 512], P('ep'), may hold values from -6 to 6
- rope_key: bfloat16 [16384, 64], P('ep'), may hold values from -6 to 6
- latent_gain: float32 [512], replicated, may hold values from 0.1 to 1.9
- w_key_up: bfloat16 [512, 1024], P(None, 'tp'), may hold values from -0.25 to 0.25
- w_value_up: bfloat16 [512, 1024], P(None, 'tp'), may hold values from -0.25 to 0.25
- query_gain: float32 [192], replicated, may hold values from 0.1 to 1.9
- key_gain: float32 [128], replicated, may hold values from 0.1 to 1.9
- rope_gain: float32 [64], replicated, may hold values from 0.1 to 1.9
- out_gain: float32 [128], replicated, may hold values from 0.1 to 1.9
- moe_tokens: bfloat16 [16384, 2048], P('ep'), may hold values from -6 to 6
- moe_gain: float32 [2048], replicated, may hold values from 0.1 to 1.9
- routes: int32 [16384, 2], P('ep'), may hold values from 0 to 63, all different within a row; in each aligned block of 64 rows (0 to 63, 64 to 127, ...) at most 3 rows name the same one
- route_weights: float32 [16384, 2], P('ep'), may hold values from 0.25 to 1
- w_gate: bfloat16 [64, 2048, 3584], P('ep', None, 'tp'), may hold values from -0.125 to 0.125
- w_up: bfloat16 [64, 2048, 3584], P('ep', None, 'tp'), may hold values from -0.125 to 0.125
- w_down: bfloat16 [64, 3584, 2048], P('ep', 'tp'), may hold values from -0.09375 to 0.09375
Outputs:
- attended: bfloat16 [16384, 1024], P('ep', 'tp')
- moe_out: bfloat16 [16384, 2048], P(('ep', 'tp'))
Inputs may be any that keep to these rules, and one draw needn't show every extreme that they name: `routes`: each row names 2 different experts of 0 to 63; in each aligned block of 64 rows no expert is named by more than 3 rows, and in some block one expert is named by exactly 3.
All inputs are finite; a program needn't handle non-finite values.
Results may differ from a plain program's by a relative error of at most 0.0071.
Values may be sent and summed in bfloat16 or wider, within the bound.
No kernel may reach another device: no remote copies, remote signals or barrier semaphores. Data moves between devices by JAX's collectives and lax.ppermute only.
A program may use at most 128 MiB of HBM per device.

v0:
```python
import functools

import jax
import jax.numpy as jnp
from jax import lax
from jax.experimental import pallas as pl
from jax.experimental.pallas import tpu as pltpu
from jax.sharding import Mesh
from jax.sharding import PartitionSpec as P


ZY = ("ep_0", "ep_1")
CORE = "ep_2"
YC = ("ep_1", "ep_2")
EP = ("ep_0", "ep_1", "ep_2")
EP_TP = ("ep_0", "ep_1", "ep_2", "tp")

EPS = 1e-06
THETA = 500000.0
LOG2E = 1.4426950408889634


def rms_norm(values, norm_gain):
    return values * lax.rsqrt(jnp.mean(values * values, axis=-1, keepdims=True) + EPS) * norm_gain


def in_hbm(x):
    return pltpu.with_memory_space_constraint(x, pltpu.HBM)


def swap_halves(v):
    lane = lax.broadcasted_iota(jnp.int32, v.shape, 1)
    return jnp.where(lane % 64 < 32, pltpu.roll(v, 96, 1), pltpu.roll(v, 32, 1))


def prepare_body(*refs):
    sources = refs[:11]
    keys_out, queries_out = refs[11:13]
    queries_ref, latent_ref, rope_ref, latent_gain, wk_ref, wv_ref, query_gain, key_gain, rope_gain, cos_ref, sin_ref = (
        refs[13:24]
    )
    sem = refs[24]
    copies = [pltpu.make_async_copy(s, d, sem.at[k]) for k, (s, d) in enumerate(zip(sources, refs[13:24]))]
    for copy in copies:
        copy.start()
    for copy in copies:
        copy.wait()
    rows = latent_ref.shape[0]
    half = rows // 2
    heads = wk_ref.shape[1] // 128
    latent = rms_norm(latent_ref[...].astype(jnp.float32), latent_gain[...]).astype(jnp.bfloat16)
    keys = jnp.dot(latent, wk_ref[...], preferred_element_type=jnp.float32)
    values = jnp.dot(latent, wv_ref[...], preferred_element_type=jnp.float32)
    for h in range(heads):
        cols = slice(h * 128, (h + 1) * 128)
        keys_out[h * rows : (h + 1) * rows, :] = rms_norm(keys[:, cols], key_gain[...]).astype(jnp.bfloat16)
        keys_out[(heads + h) * rows : (heads + h + 1) * rows, :] = values[:, cols].astype(jnp.bfloat16)
    cos = cos_ref[...]
    sin = sin_ref[...]
    lane = lax.broadcasted_iota(jnp.int32, (half, 128), 1)
    rope = rms_norm(rope_ref[...].astype(jnp.float32), rope_gain[...])
    rope = jnp.concatenate([rope[:half], rope[half:]], axis=1)
    cos_k = jnp.where(lane < 64, cos[:half], cos[half:])
    sin_k = jnp.where(lane < 64, sin[:half], sin[half:])
    keys_out[2 * heads * rows :, :] = (rope * cos_k + swap_halves(rope) * sin_k).astype(jnp.bfloat16)
    ropes = []
    for h in range(heads):
        query = rms_norm(queries_ref[:, h * 192 : (h + 1) * 192].astype(jnp.float32), query_gain[...])
        queries_out[h * rows : (h + 1) * rows, :] = query[:, :128].astype(jnp.bfloat16)
        ropes.append(query[:, 128:])
    rope = jnp.concatenate(ropes, axis=1)
    queries_out[heads * rows :, :] = (rope * cos + swap_halves(rope) * sin).astype(jnp.bfloat16)


def prepare(queries, kv_latent, rope_key, latent_gain, w_key_up, w_value_up, query_gain, key_gain, rope_gain, positions):
    rows = queries.shape[0]
    rope_dim = rope_key.shape[1]
    freqs = 1.0 / THETA ** (jnp.arange(0, rope_dim, 2, dtype=jnp.float32) / rope_dim)
    lane = jnp.arange(128, dtype=jnp.int32)
    angles = positions.astype(jnp.float32)[:, None] * jnp.tile(freqs, 4)[None, :]
    sign = jnp.where(lane % 64 < 32, -1.0, 1.0)[None, :]
    args = (
        queries, kv_latent, rope_key, latent_gain.reshape(1, -1), w_key_up, w_value_up, query_gain.reshape(1, -1),
        key_gain.reshape(1, -1), rope_gain.reshape(1, -1), jnp.cos(angles), jnp.sin(angles) * sign,
    )
    return pl.pallas_call(
        prepare_body,
        in_specs=[pl.BlockSpec(memory_space=pltpu.HBM)] * len(args),
        out_specs=[pl.BlockSpec(memory_space=pltpu.VMEM)] * 2,
        scratch_shapes=[pltpu.VMEM(a.shape, a.dtype) for a in args] + [pltpu.SemaphoreType.DMA((len(args),))],
        out_shape=[
            jax.ShapeDtypeStruct((rows * 9 // 2, 128), jnp.bfloat16),
            jax.ShapeDtypeStruct((rows * 3, 128), jnp.bfloat16),
        ],
        cost_estimate=pl.CostEstimate(flops=rows * 512 * 512 * 2, bytes_accessed=2 << 20, transcendentals=0),
        compiler_params=pltpu.CompilerParams(vmem_limit_bytes=16 << 20),
        name="prepare",
    )(*[in_hbm(a) for a in args])


def flash_body(groups, rows, scale, pieces, at_ref, *refs):
    q_hbm = refs[:pieces]
    kv_hbm, out_ref, kt_ref, vt_ref, all_q_ref, kv_ref, sem = refs[pieces:]
    tile = pl.program_id(0)
    group = at_ref[0]
    place = at_ref[1]
    heads = 2
    half = rows // 2
    per = kv_ref.shape[0] // groups

    @pl.when(tile == 0)
    def _():
        lane = lax.broadcasted_iota(jnp.int32, (rows, 128), 1)
        copies = []
        for g in range(groups):
            part = pl.ds(g * per, per)
            copies.append(pltpu.make_async_copy(kv_hbm.at[part], kv_ref.at[part], sem.at[g]))
        first = 0
        for k, piece in enumerate(q_hbm):
            part = pl.ds(first, piece.shape[0])
            copies.append(pltpu.make_async_copy(piece, all_q_ref.at[part], sem.at[groups + k]))
            first += piece.shape[0]
        for copy in copies:
            copy.start()
        for g in range(groups):
            copies[g].wait()
            base = g * per
            seen = jnp.where(g <= group, 1.0, 0.0).astype(jnp.float32)
            rope = kv_ref[base + 2 * heads * rows : base + per, :].astype(jnp.float32)
            turned = pltpu.roll(rope, 64, 1)
            low = jnp.where(lane < 64, jnp.concatenate([rope, turned], axis=0), 0.0).astype(jnp.bfloat16)
            high = jnp.where(lane >= 64, jnp.concatenate([turned, rope], axis=0), 0.0).astype(jnp.bfloat16)
            for h in range(heads):
                kt_ref[g * heads + h, :, :128] = kv_ref[base + h * rows : base + (h + 1) * rows, :]
                kt_ref[g * heads + h, :, 128:] = low if h == 0 else high
                vals = kv_ref[base + (heads + h) * rows : base + (heads + h + 1) * rows, :].astype(jnp.float32)
                vt_ref[g * heads + h, :, :128] = (vals * seen).astype(jnp.bfloat16)
                vt_ref[g * heads + h, :, 128:] = jnp.full((rows, 128), seen, jnp.float32).astype(jnp.bfloat16)

        for copy in copies[groups:]:
            copy.wait()

    q_ref = all_q_ref.at[pl.ds(pl.multiple_of(tile * 3 * rows, 3 * rows), 3 * rows)]
    q_rope = q_ref[heads * rows :, :]
    sums = []
    for h in range(heads):
        query = jnp.concatenate([q_ref[h * rows : (h + 1) * rows, :], q_rope], axis=1)
        total = None
        for k in range(groups):
            at = ((group + k) % groups) * heads + h
            scores = lax.dot_general(
                query, kt_ref[at], (((1,), (1,)), ((), ())), preferred_element_type=jnp.float32
            )
            soft = jnp.exp2(scores * (scale * LOG2E))
            if k == 0:
                qi = lax.broadcasted_iota(jnp.int32, soft.shape, 0) + (at_ref[2 + tile] - place) * rows
                ki = lax.broadcasted_iota(jnp.int32, soft.shape, 1)
                soft = jnp.where(qi >= ki, soft, 0.0)
            part = jnp.dot(soft.astype(jnp.bfloat16), vt_ref[at], preferred_element_type=jnp.float32)
            total = part if total is None else total + part
        out_ref[h * rows : (h + 1) * rows, :] = total[:, :128].astype(jnp.bfloat16)
        for t in range(2):
            den = total[t * half : (t + 1) * half, 128:]
            ri = lax.broadcasted_iota(jnp.int32, den.shape, 0)
            ci = lax.broadcasted_iota(jnp.int32, den.shape, 1)
            sums.append(jnp.sum(jnp.where(ri == ci, den, 0.0), axis=0, keepdims=True))
    sums = jnp.concatenate(sums + [jnp.zeros((4, 128), jnp.float32)], axis=0)
    high = sums.astype(jnp.bfloat16).astype(jnp.float32)
    low = sums - high
    out_ref[heads * rows :, :] = jnp.concatenate([high, low], axis=0).astype(jnp.bfloat16)


def flash(at, pieces, keys, groups, scale):
    rows = keys.shape[0] // groups * 2 // 9
    q_rows = sum(p.shape[0] for p in pieces)
    tiles = q_rows // (3 * rows)
    out_rows = 2 * rows + 16
    grid_spec = pltpu.PrefetchScalarGridSpec(
        num_scalar_prefetch=1,
        grid=(tiles,),
        in_specs=[
            pl.BlockSpec(memory_space=pltpu.HBM),
        ]
        * (len(pieces) + 1),
        out_specs=pl.BlockSpec((out_rows, 128), lambda s, i: (i[2 + s], 0)),
        scratch_shapes=[
            pltpu.VMEM((2 * groups, rows, 256), jnp.bfloat16),
            pltpu.VMEM((2 * groups, rows, 256), jnp.bfloat16),
            pltpu.VMEM((q_rows, 128), jnp.bfloat16),
            pltpu.VMEM(keys.shape, jnp.bfloat16),
            pltpu.SemaphoreType.DMA((groups + len(pieces),)),
        ],
    )
    pairs = 2 * rows * rows * groups * tiles
    return pl.pallas_call(
        functools.partial(flash_body, groups, rows, scale, len(pieces)),
        grid_spec=grid_spec,
        out_shape=jax.ShapeDtypeStruct((tiles * out_rows, 128), jnp.bfloat16),
        cost_estimate=pl.CostEstimate(flops=pairs * 1024, bytes_accessed=4 << 20, transcendentals=pairs),
        compiler_params=pltpu.CompilerParams(dimension_semantics=("arbitrary",), vmem_limit_bytes=24 << 20),
        name="flash",
    )(at, *[in_hbm(p) for p in pieces], in_hbm(keys))


def finish_body(count, in_ref, gain_ref, out_ref):
    per = in_ref.shape[0] // count
    rows = out_ref.shape[0]
    half = rows // 2
    total = in_ref[:per, :].astype(jnp.float32)
    for k in range(1, count):
        total = total + in_ref[k * per : (k + 1) * per, :].astype(jnp.float32)
    sums = total[2 * rows : 2 * rows + 8] + total[2 * rows + 8 : 2 * rows + 16]
    ri = lax.broadcasted_iota(jnp.int32, (half, 128), 0)
    ci = lax.broadcasted_iota(jnp.int32, (half, 128), 1)
    for h in range(2):
        for t in range(2):
            den = jnp.sum(jnp.where(ri == ci, sums[2 * h + t : 2 * h + t + 1], 0.0), axis=1, keepdims=True)
            mixed = total[h * rows + t * half : h * rows + (t + 1) * half] / den
            out_ref[t * half : (t + 1) * half, h * 128 : (h + 1) * 128] = rms_norm(mixed, gain_ref[...]).astype(
                jnp.bfloat16
            )


def finish(parts, out_gain, count, rows):
    whole = pl.BlockSpec(memory_space=pltpu.VMEM)
    return pl.pallas_call(
        functools.partial(finish_body, count),
        in_specs=[whole, whole],
        out_specs=whole,
        out_shape=jax.ShapeDtypeStruct((rows, 256), jnp.bfloat16),
        compiler_params=pltpu.CompilerParams(vmem_limit_bytes=16 << 20),
        name="finish",
    )(parts, out_gain.reshape(1, -1))


def mlp_body(pieces, *refs):
    x_refs = refs[:pieces]
    wg_ref, wu_ref, wd_ref = refs[pieces : pieces + 3]
    out_refs = refs[pieces + 3 :]
    x = jnp.concatenate([r[...] for r in x_refs], axis=0)
    gate = jnp.dot(x, wg_ref[...], preferred_element_type=jnp.float32)
    up = jnp.dot(x, wu_ref[...], preferred_element_type=jnp.float32)
    hidden = (gate / (1.0 + jnp.exp(-gate)) * up).astype(jnp.bfloat16)
    y = jnp.dot(hidden, wd_ref[...], preferred_element_type=jnp.float32)
    first = 0
    for ref in out_refs:
        ref[...] = y[first : first + ref.shape[0]].astype(ref.dtype)
        first += ref.shape[0]


def mlp(xs, w_gate, w_up, w_down):
    rows = sum(x.shape[0] for x in xs)
    dim, hid = w_gate.shape
    whole = pl.BlockSpec(memory_space=pltpu.VMEM)
    dtypes = [jnp.float32] + [jnp.bfloat16] * (len(xs) - 1)
    return pl.pallas_call(
        functools.partial(mlp_body, len(xs)),
        in_specs=[whole] * (len(xs) + 3),
        out_specs=[whole] * len(xs),
        out_shape=[jax.ShapeDtypeStruct(x.shape, d) for x, d in zip(xs, dtypes)],
        cost_estimate=pl.CostEstimate(
            flops=2 * rows * dim * hid * 3, bytes_accessed=3 * dim * hid * 2, transcendentals=rows * hid
        ),
        compiler_params=pltpu.CompilerParams(vmem_limit_bytes=16 << 20),
        name="mlp",
    )(*xs, w_gate, w_up, w_down)


def shifted(x, axis, by):
    count = lax.axis_size(axis)
    return lax.ppermute(x, axis, [(i, (i + by) % count) for i in range(count)])


def send_body(capacity, at_ref, routes_ref, tokens_ref, gain_ref, near_out, far_out, hits_out):
    core = at_ref[1]
    rows = tokens_ref.shape[0]
    lane = lax.broadcasted_iota(jnp.int32, (rows, 128), 1)
    normed = rms_norm(tokens_ref[...].astype(jnp.float32), gain_ref[...]).astype(jnp.bfloat16)
    chosen = [routes_ref[:, k : k + 1] for k in range(2)]
    named = [(c == lane).astype(jnp.float32) for c in chosen]
    before = lax.broadcasted_iota(jnp.int32, (rows, rows), 1) < lax.broadcasted_iota(jnp.int32, (rows, rows), 0)
    count = jnp.dot(
        before.astype(jnp.float32).astype(jnp.bfloat16),
        (named[0] + named[1]).astype(jnp.bfloat16),
        preferred_element_type=jnp.float32,
    )
    sends = [jnp.zeros((rows, 128), jnp.float32), jnp.zeros((rows, 128), jnp.float32)]
    for k in range(2):
        rank = jnp.sum(count * named[k], axis=1, keepdims=True).astype(jnp.int32)
        away = (chosen[k] & 1) ^ core
        slot = (chosen[k] >> 1) * capacity + rank
        for side in range(2):
            hit = ((slot == lane) & (away == side)).astype(jnp.float32)
            hits_out[side, k] = hit.astype(jnp.bfloat16)
            sends[side] = sends[side] + hit
    for side, ref in enumerate((near_out, far_out)):
        moved = lax.dot_general(
            sends[side].astype(jnp.bfloat16), normed, (((0,), (0,)), ((), ())), preferred_element_type=jnp.float32
        )
        ref[...] = moved[: ref.shape[0]].astype(jnp.bfloat16)


def send_rows(part, moe_tokens, moe_gain, routes, part_rows, capacity, half):
    dim = moe_tokens.shape[1]
    at = jnp.stack([part, lax.axis_index(CORE)]).astype(jnp.int32)
    grid_spec = pltpu.PrefetchScalarGridSpec(
        num_scalar_prefetch=1,
        grid=(1,),
        in_specs=[
            pl.BlockSpec((part_rows, 2), lambda s, i: (i[0], 0)),
            pl.BlockSpec((part_rows, dim), lambda s, i: (i[0], 0)),
            pl.BlockSpec((1, dim), lambda s, i: (0, 0)),
        ],
        out_specs=[
            pl.BlockSpec((half, dim), lambda s, i: (0, 0)),
            pl.BlockSpec((half, dim), lambda s, i: (0, 0)),
            pl.BlockSpec((2, 2, part_rows, 128), lambda s, i: (0, 0, 0, 0)),
        ],
    )
    return pl.pallas_call(
        functools.partial(send_body, capacity),
        grid_spec=grid_spec,
        out_shape=[
            jax.ShapeDtypeStruct((half, dim), jnp.bfloat16),
            jax.ShapeDtypeStruct((half, dim), jnp.bfloat16),
            jax.ShapeDtypeStruct((2, 2, part_rows, 128), jnp.bfloat16),
        ],
        compiler_params=pltpu.CompilerParams(vmem_limit_bytes=16 << 20),
        name="send",
    )(at, in_hbm(routes), in_hbm(moe_tokens), in_hbm(moe_gain.reshape(1, -1)))


def experts_part(moe_tokens, moe_gain, routes, route_weights, w_gate, w_up, w_down, queries, attend):
    n_rows = moe_tokens.shape[0]
    top_count = routes.shape[1]
    quarters = lax.axis_size("tp")
    part_rows = n_rows // quarters
    experts = lax.axis_size(EP)
    zy_count = lax.axis_size(ZY)
    capacity = (3 * top_count * part_rows + 2 * experts - 1) // (2 * experts)
    my_part = lax.axis_index("tp")
    own_weights = lax.dynamic_slice_in_dim(route_weights, my_part * part_rows, part_rows, 0)
    half = zy_count * capacity
    near, far, hits = send_rows(my_part, moe_tokens, moe_gain, routes, part_rows, capacity, half)
    far = shifted(far, CORE, 1)

    def dispatch(rows):
        blocks = rows.reshape(zy_count, -1, 128)
        return lax.all_to_all(blocks, ZY, 0, 0, tiled=True).reshape(rows.shape)

    def spread(rows):
        return [rows, shifted(rows, "tp", 1), shifted(rows, "tp", -1), shifted(rows, "tp", 2)]

    def total(parts):
        back = [parts[0], shifted(parts[1], "tp", -1), shifted(parts[2], "tp", 1), shifted(parts[3], "tp", 2)]
        whole = back[0]
        for part in back[1:]:
            whole = whole + part.astype(jnp.float32)
        return whole.astype(jnp.bfloat16)

    near_in = dispatch(near)
    far_in = dispatch(far)
    near_x = spread(near_in)
    far_x = spread(far_in)
    near_y = mlp(near_x, w_gate[0], w_up[0], w_down[0])
    far_y = mlp(far_x, w_gate[0], w_up[0], w_down[0])
    parts = attend(queries)
    near_sum = total(near_y)
    far_sum = total(far_y)
    near_back = dispatch(near_sum)
    far_back = dispatch(far_sum)
    far_back = shifted(far_back, CORE, 1)
    mixed = jnp.zeros((part_rows, near_back.shape[1]), jnp.float32)
    for k in range(top_count):
        picked = jnp.dot(hits[0, k, :, :half], near_back, preferred_element_type=jnp.float32) + jnp.dot(
            hits[1, k, :, :half], far_back, preferred_element_type=jnp.float32
        )
        mixed = mixed + picked * own_weights[:, k : k + 1]
    return mixed.astype(jnp.bfloat16), parts


def on_device(
    queries,
    kv_latent,
    rope_key,
    latent_gain,
    w_key_up,
    w_value_up,
    query_gain,
    key_gain,
    rope_gain,
    out_gain,
    moe_tokens,
    moe_gain,
    routes,
    route_weights,
    w_gate,
    w_up,
    w_down,
):
    tok_rows = queries.shape[0]
    index = lax.axis_index(EP)
    positions = index * tok_rows + jnp.arange(tok_rows, dtype=jnp.int32)

    def attend(raw_queries):
        keys, own = prepare(
            raw_queries, kv_latent, rope_key, latent_gain, w_key_up, w_value_up, query_gain, key_gain, rope_gain, positions
        )
        keys = lax.all_gather(keys, "ep_0", axis=0, tiled=True)
        pair = jnp.concatenate([own, shifted(own, CORE, 1)], axis=0)
        shifts = (0, 1, 3, 2)
        pieces = [pair] + [shifted(pair, "ep_1", s) for s in shifts[1:]]
        row = lax.axis_index("ep_1")
        core = lax.axis_index(CORE)
        places = [((row - s) & 3) * 2 + (core ^ away) for s in shifts for away in (0, 1)]
        at = jnp.stack([lax.axis_index("ep_0"), row * 2 + core] + places).astype(jnp.int32)
        return flash(at, pieces, keys, lax.axis_size("ep_0"), query_gain.shape[0] ** -0.5)

    moe_out, parts = experts_part(
        moe_tokens, moe_gain, routes, route_weights, w_gate, w_up, w_down, queries, attend
    )
    parts = lax.psum_scatter(parts, YC, scatter_dimension=0, tiled=True)
    attended = finish(parts, out_gain, 1, tok_rows)
    return (attended, moe_out)


def solution(mesh):
    finer = Mesh(mesh.devices.reshape(8, 4, 2, mesh.shape["tp"]), ("ep_0", "ep_1", "ep_2", "tp"))
    placed = (
        P(EP, "tp"),
        P(EP, None),
        P(EP, None),
        P(),
        P(None, "tp"),
        P(None, "tp"),
        P(),
        P(),
        P(),
        P(),
        P(EP, None),
        P(),
        P(EP, None),
        P(EP, None),
        P(EP, None, "tp"),
        P(EP, None, "tp"),
        P(EP, "tp", None),
    )

    return jax.shard_map(
        on_device,
        mesh=finer,
        in_specs=placed,
        out_specs=(P(EP, "tp"), P(EP_TP, None)),
        check_vma=False,
    )
```

profile of v0, /device:TPU:6, one launch (start us, length us, event | category | flops | bytes accessed | tf_op | source)
XLA Modules:
  0.0 193.8 jit_solution(8793715920295731449)
XLA Ops:
  7.3 1.5 copy.19.refs_2_
  8.8 1.2 fusion.4
  10.1 2.8 %prepare.1 = (bf16[1152,128]{1,0:T(8,128)(2,1)}, bf16[768,128]{1,0:T(8,128)(2,1)S(1)}) custom-call(bf16[256,384]{1,0:T(8,128)(2,1)} %refs_0_.1, bf16[256,512]{1,0:T(8,128)(2,1)} %refs_1_.1, bf16[256,64]{1,0:T(8,128)(2,1)} %copy.19.refs_2_, f32[1,512]{1,0:T(1,128)} %bitcast.49, bf16[512,256]{1,0:T(8,128)(2,1)} %refs_4_.1, bf16[512,256]{1,0:T(8,128)(2,1)} %refs_5_.1, ...), custom_call_target="tpu_custom_call" | custom-call | flops 134217728 | bytes 2097152 | tf_op jit(solution)/shard_map/prepare/pallas_call | solution.py:86
  12.9 1.5 copy.20.routes_ref
  14.4 2.4 %send.1 = (bf16[96,2048]{1,0:T(8,128)(2,1)S(1)}, bf16[96,2048]{1,0:T(8,128)(2,1)S(1)}, bf16[2,2,64,128]{3,2,1,0:T(8,128)(2,1)S(1)}) custom-call(s32[2]{0:T(128)S(1)} %pad_add_fusion.at_ref, s32[256,2]{1,0:T(8,128)} %copy.20.routes_ref, bf16[256,2048]{1,0:T(8,128)(2,1)} %tokens_ref.1, f32[1,2048]{1,0:T(1,128)} %bitcast.48), custom_call_target="tpu_custom_call" | custom-call | tf_op jit(solution)/shard_map/send/pallas_call | solution.py:320
  16.8 0.9 reshape.75
  17.8 11.5 %all-to-all-start = ((bf16[32,48,128]{2,1,0:T(8,128)(2,1)}), bf16[32,48,128]{2,1,0:T(8,128)(2,1)S(1)}, u32[]{:S(2)}, u32[]{:S(2)}) async-start(bf16[32,48,128]{2,1,0:T(8,128)(2,1)} %reshape.75), calls=%async_computation.1 | async-start | bytes 786432 | tf_op jit(solution)/shard_map/all_to_all | solution.py:349
  29.3 19.7 %all-to-all-done = bf16[32,48,128]{2,1,0:T(8,128)(2,1)S(1)} async-done(((bf16[32,48,128]{2,1,0:T(8,128)(2,1)}), bf16[32,48,128]{2,1,0:T(8,128)(2,1)S(1)}, u32[]{:S(2)}, u32[]{:S(2)}) %all-to-all-start) | async-done | bytes 393248 | tf_op jit(solution)/shard_map/all_to_all | solution.py:349
  49.1 0.2 reshape.76.refs_0_
  49.2 0.6 collective-permute-start.4
  49.8 1.5 collective-permute-start.5
  51.3 1.4 collective-permute-start.6
  52.7 0.9 reshape.79
  53.7 4.6 %all-to-all-start.2 = ((bf16[32,48,128]{2,1,0:T(8,128)(2,1)}), bf16[32,48,128]{2,1,0:T(8,128)(2,1)}, u32[]{:S(2)}, u32[]{:S(2)}) async-start(bf16[32,48,128]{2,1,0:T(8,128)(2,1)} %reshape.79), calls=%async_computation.3 | async-start | bytes 786432 | tf_op jit(solution)/shard_map/all_to_all | solution.py:349
  58.3 3.0 %collective-permute-done.4.refs_1_ = bf16[96,2048]{1,0:T(8,128)(2,1)S(1)} collective-permute-done((bf16[96,2048]{1,0:T(8,128)(2,1)S(1)}, bf16[96,2048]{1,0:T(8,128)(2,1)S(1)}, u32[]{:S(2)}, u32[]{:S(2)}) %collective-permute-start.4) | collective-permute-done | bytes 393248 | tf_op jit(solution)/shard_map/ppermute | solution.py:271
  61.3 6.9 %collective-permute-done.5.refs_2_ = bf16[96,2048]{1,0:T(8,128)(2,1)S(1)} collective-permute-done((bf16[96,2048]{1,0:T(8,128)(2,1)S(1)}, bf16[96,2048]{1,0:T(8,128)(2,1)S(1)}, u32[]{:S(2)}, u32[]{:S(2)}) %collective-permute-start.5) | collective-permute-done | bytes 393248 | tf_op jit(solution)/shard_map/ppermute | solution.py:271
  68.2 0.7 copy-done.11
  69.0 2.0 %copy-done.3 = bf16[1,2048,896]{2,1,0:T(8,128)(2,1)S(1)} copy-done((bf16[1,2048,896]{2,1,0:T(8,128)(2,1)S(1)}, bf16[1,2048,896]{2,1,0:T(8,128)(2,1)}, u32[]{:S(2)}) %copy-start.3) | copy-done | bytes 3670040
  71.0 2.0 %copy-done.5 = bf16[1,2048,896]{2,1,0:T(8,128)(2,1)S(1)} copy-done((bf16[1,2048,896]{2,1,0:T(8,128)(2,1)S(1)}, bf16[1,2048,896]{2,1,0:T(8,128)(2,1)}, u32[]{:S(2)}) %copy-start.5) | copy-done | bytes 3670040
  73.1 2.0 %copy-done.7 = bf16[1,896,2048]{2,1,0:T(8,128)(2,1)S(1)} copy-done((bf16[1,896,2048]{2,1,0:T(8,128)(2,1)S(1)}, bf16[1,896,2048]{2,1,0:T(8,128)(2,1)}, u32[]{:S(2)}) %copy-start.7) | copy-done | bytes 3670040
  75.1 1.0 copy-done.12
  76.1 5.1 %mlp.2 = (f32[96,2048]{1,0:T(8,128)S(1)}, bf16[96,2048]{1,0:T(8,128)(2,1)S(1)}, bf16[96,2048]{1,0:T(8,128)(2,1)S(1)}, bf16[96,2048]{1,0:T(8,128)(2,1)S(1)}) custom-call(bf16[96,2048]{1,0:T(8,128)(2,1)S(1)} %reshape.76.refs_0_, bf16[96,2048]{1,0:T(8,128)(2,1)S(1)} %collective-permute-done.4.refs_1_, bf16[96,2048]{1,0:T(8,128)(2,1)S(1)} %collective-permute-done.5.refs_2_, ...), custom_call_target="tpu_custom_call" | custom-call | flops 4227858432 | bytes 11010048 | tf_op jit(solution)/shard_map/mlp/pallas_call | solution.py:256
  81.2 2.0 %collective-permute-start.9 = (bf16[96,2048]{1,0:T(8,128)(2,1)S(1)}, bf16[96,2048]{1,0:T(8,128)(2,1)}, u32[]{:S(2)}, u32[]{:S(2)}) collective-permute-start(bf16[96,2048]{1,0:T(8,128)(2,1)S(1)} %get-tuple-element.22), channel_id=1, source_target_pairs={{0,2},{1,3},{2,0},{3,1},{4,6},{5,7},{6,4},{7,5},{8,10},{9,11},{10,... | collective-permute-start | bytes 1179656 | tf_op jit(solution)/shard_map/ppermute | solution.py:271
  83.2 0.2 collective-permute-start.8
  83.4 1.8 collective-permute-start.7
  85.3 0.7 constant_dynamic-update-slice_fusion.1
  86.0 0.7 collective-permute-done
  86.6 0.7 constant_dynamic-update-slice_fusion.refs_0_
  87.3 1.5 collective-permute-start.1
  88.9 1.7 collective-permute-start.2
  90.6 1.2 reshape.80.refs_0_
  91.7 3.1 %collective-permute-done.9 = bf16[96,2048]{1,0:T(8,128)(2,1)} collective-permute-done((bf16[96,2048]{1,0:T(8,128)(2,1)S(1)}, bf16[96,2048]{1,0:T(8,128)(2,1)}, u32[]{:S(2)}, u32[]{:S(2)}) %collective-permute-start.9) | collective-permute-done | bytes 393248 | tf_op jit(solution)/shard_map/ppermute | solution.py:271
  94.9 1.3 collective-permute-start.11
  96.2 5.8 %collective-permute-done.8 = bf16[96,2048]{1,0:T(8,128)(2,1)} collective-permute-done((bf16[96,2048]{1,0:T(8,128)(2,1)S(1)}, bf16[96,2048]{1,0:T(8,128)(2,1)}, u32[]{:S(2)}, u32[]{:S(2)}) %collective-permute-start.8) | collective-permute-done | bytes 393248 | tf_op jit(solution)/shard_map/ppermute | solution.py:271
  101.9 1.4 collective-permute-start.13
  103.3 1.4 add_convert_fusion.1
  104.8 0.9 reshape.77
  105.7 5.3 %all-to-all-start.1 = ((bf16[32,48,128]{2,1,0:T(8,128)(2,1)}), bf16[32,48,128]{2,1,0:T(8,128)(2,1)}, u32[]{:S(2)}, u32[]{:S(2)}) async-start(bf16[32,48,128]{2,1,0:T(8,128)(2,1)} %reshape.77), calls=%async_computation.2 | async-start | bytes 786432 | tf_op jit(solution)/shard_map/all_to_all | solution.py:349
  111.1 3.3 %collective-permute-start.3 = (bf16[1536,128]{1,0:T(8,128)(2,1)}, bf16[1536,128]{1,0:T(8,128)(2,1)}, u32[]{:S(2)}, u32[]{:S(2)}) collective-permute-start(bf16[1536,128]{1,0:T(8,128)(2,1)} %constant_dynamic-update-slice_fusion.refs_0_), channel_id=1, source_target_pairs={{0,16},{8,24},{16,0},{24,8},{1,17},{9,25},{17,1},{25,9},{2,18},{10... | collective-permute-start | bytes 1179656 | tf_op jit(solution)/shard_map/ppermute | solution.py:271
  114.4 5.4 %collective-permute-done.13.refs_3_ = bf16[96,2048]{1,0:T(8,128)(2,1)S(1)} collective-permute-done((bf16[96,2048]{1,0:T(8,128)(2,1)S(1)}, bf16[96,2048]{1,0:T(8,128)(2,1)S(1)}, u32[]{:S(2)}, u32[]{:S(2)}) %collective-permute-start.13) | collective-permute-done | bytes 393248 | tf_op jit(solution)/shard_map/ppermute | solution.py:271
  119.8 0.8 copy-done.9
  120.6 2.0 %copy-done.4 = bf16[1,2048,896]{2,1,0:T(8,128)(2,1)S(1)} copy-done((bf16[1,2048,896]{2,1,0:T(8,128)(2,1)S(1)}, bf16[1,2048,896]{2,1,0:T(8,128)(2,1)}, u32[]{:S(2)}) %copy-start.4) | copy-done | bytes 3670040
  122.6 2.0 %copy-done.6 = bf16[1,2048,896]{2,1,0:T(8,128)(2,1)S(1)} copy-done((bf16[1,2048,896]{2,1,0:T(8,128)(2,1)S(1)}, bf16[1,2048,896]{2,1,0:T(8,128)(2,1)}, u32[]{:S(2)}) %copy-start.6) | copy-done | bytes 3670040
  124.7 2.0 %copy-done.8 = bf16[1,896,2048]{2,1,0:T(8,128)(2,1)S(1)} copy-done((bf16[1,896,2048]{2,1,0:T(8,128)(2,1)S(1)}, bf16[1,896,2048]{2,1,0:T(8,128)(2,1)}, u32[]{:S(2)}) %copy-start.8) | copy-done | bytes 3670040
  126.7 1.0 copy-done.10
  127.7 5.1 %mlp.3 = (f32[96,2048]{1,0:T(8,128)S(1)}, bf16[96,2048]{1,0:T(8,128)(2,1)S(1)}, bf16[96,2048]{1,0:T(8,128)(2,1)S(1)}, bf16[96,2048]{1,0:T(8,128)(2,1)S(1)}) custom-call(bf16[96,2048]{1,0:T(8,128)(2,1)S(1)} %reshape.80.refs_0_, bf16[96,2048]{1,0:T(8,128)(2,1)S(1)} %collective-permute-done.11.refs_1_, bf16[96,2048]{1,0:T(8,128)(2,1)S(1)} %collective-permute-done.12.refs_2_, ...), custom_call_target="tpu_custom_call" | custom-call | flops 4227858432 | bytes 11010048 | tf_op jit(solution)/shard_map/mlp/pallas_call | solution.py:256
  132.8 0.3 collective-permute-start.16
  133.1 2.0 %collective-permute-start.14 = (bf16[96,2048]{1,0:T(8,128)(2,1)S(1)}, bf16[96,2048]{1,0:T(8,128)(2,1)S(1)}, u32[]{:S(2)}, u32[]{:S(2)}) collective-permute-start(bf16[96,2048]{1,0:T(8,128)(2,1)S(1)} %get-tuple-element.25), channel_id=1, source_target_pairs={{0,3},{1,0},{2,1},{3,2},{4,7},{5,4},{6,5},{7,6},{8,11},{9,8},{10,9... | collective-permute-start | bytes 1179656 | tf_op jit(solution)/shard_map/ppermute | solution.py:271
  135.1 15.4 %flash.1 = bf16[4224,128]{1,0:T(8,128)(2,1)} custom-call(s32[10]{0:T(128)S(1)} %stack.52.at_ref, bf16[1536,128]{1,0:T(8,128)(2,1)} %constant_dynamic-update-slice_fusion.refs_0_, bf16[1536,128]{1,0:T(8,128)(2,1)} %collective-permute-done.1.refs_1_, bf16[1536,128]{1,0:T(8,128)(2,1)} %collective-permute-done.2.refs_2_, ...), custom_call_target="tpu_custom_call" | custom-call | flops 8589934592 | bytes 4194304 | tf_op jit(solution)/shard_map/flash/pallas_call | solution.py:195
  150.6 1.6 collective-permute-done.14
  152.2 0.2 add_convert_fusion
  152.4 0.9 reshape.81
  153.3 7.0 %all-to-all-start.3 = ((bf16[32,48,128]{2,1,0:T(8,128)(2,1)}), bf16[32,48,128]{2,1,0:T(8,128)(2,1)S(1)}, u32[]{:S(2)}, u32[]{:S(2)}) async-start(bf16[32,48,128]{2,1,0:T(8,128)(2,1)} %reshape.81), calls=%async_computation.4 | async-start | bytes 786432 | tf_op jit(solution)/shard_map/all_to_all | solution.py:349
  160.4 1.2 reshape.78
  161.6 14.2 %all-to-all-done.3 = bf16[32,48,128]{2,1,0:T(8,128)(2,1)S(1)} async-done(((bf16[32,48,128]{2,1,0:T(8,128)(2,1)}), bf16[32,48,128]{2,1,0:T(8,128)(2,1)S(1)}, u32[]{:S(2)}, u32[]{:S(2)}) %all-to-all-start.3) | async-done | bytes 393248 | tf_op jit(solution)/shard_map/all_to_all | solution.py:349
  175.8 0.2 reshape.82
  176.1 0.2 fusion.9
  176.3 0.2 fusion.6
  176.5 1.3 collective-permute-done.17
  177.8 0.2 fusion.2
  178.0 0.9 fusion.3
  178.9 6.3 %reduce-scatter.2.cloned.1.call-done.in_ref = bf16[528,128]{1,0:T(8,128)(2,1)} async-done(((bf16[4224,128]{1,0:T(8,128)(2,1)}), bf16[528,128]{1,0:T(8,128)(2,1)}) %reduce-scatter.2.cloned.1.call-update) | async-done | bytes 135184 | tf_op jit(solution)/shard_map/reduce_scatter | solution.py:422
  185.2 0.9 copy-done.1
  186.1 0.9 finish.1
  (46 shorter events, 0.7 us)
Async XLA Ops:
  7.2 153.2 %copy-start = (f32[256,2]{0,1:T(2,128)S(1)}, f32[256,2]{0,1:T(2,128)}, u32[]{:S(2)}) copy-start(f32[256,2]{0,1:T(2,128)} %param.30) | copy-start | bytes 6148
  7.2 127.9 %all-gather.2.cloned.1.call-start = ((), (), s32[]{:S(2)}) async-start(), calls=%async_computation.5 | async-start | bytes 2654208 | tf_op jit(solution)/shard_map/all_gather | solution.py:409
  17.8 31.3 %all-to-all-start = ((bf16[32,48,128]{2,1,0:T(8,128)(2,1)}), bf16[32,48,128]{2,1,0:T(8,128)(2,1)S(1)}, u32[]{:S(2)}, u32[]{:S(2)}) async-start(bf16[32,48,128]{2,1,0:T(8,128)(2,1)} %reshape.75), calls=%async_computation.1 | async-start | bytes 786432 | tf_op jit(solution)/shard_map/all_to_all | solution.py:349
  29.2 23.5 %collective-permute-start.10 = (bf16[96,2048]{1,0:T(8,128)(2,1)S(1)}, bf16[96,2048]{1,0:T(8,128)(2,1)S(1)}, u32[]{:S(2)}, u32[]{:S(2)}) collective-permute-start(bf16[96,2048]{1,0:T(8,128)(2,1)S(1)} %get-tuple-element.23), channel_id=1, source_target_pairs={{0,4},{4,0},{1,5},{5,1},{2,6},{6,2},{3,7},{7,3},{8,12},{12,8},{9,1... | collective-permute-start | bytes 1179656 | tf_op jit(solution)/shard_map/ppermute | solution.py:271
  49.2 12.1 %collective-permute-start.4 = (bf16[96,2048]{1,0:T(8,128)(2,1)S(1)}, bf16[96,2048]{1,0:T(8,128)(2,1)S(1)}, u32[]{:S(2)}, u32[]{:S(2)}) collective-permute-start(bf16[96,2048]{1,0:T(8,128)(2,1)S(1)} %reshape.76.refs_0_), channel_id=1, source_target_pairs={{0,1},{1,2},{2,3},{3,0},{4,5},{5,6},{6,7},{7,4},{8,9},{9,10},{10,1... | collective-permute-start | bytes 1179656 | tf_op jit(solution)/shard_map/ppermute | solution.py:271
  49.8 18.4 %collective-permute-start.5 = (bf16[96,2048]{1,0:T(8,128)(2,1)S(1)}, bf16[96,2048]{1,0:T(8,128)(2,1)S(1)}, u32[]{:S(2)}, u32[]{:S(2)}) collective-permute-start(bf16[96,2048]{1,0:T(8,128)(2,1)S(1)} %reshape.76.refs_0_), channel_id=1, source_target_pairs={{0,3},{1,0},{2,1},{3,2},{4,7},{5,4},{6,5},{7,6},{8,11},{9,8},{10,9... | collective-permute-start | bytes 1179656 | tf_op jit(solution)/shard_map/ppermute | solution.py:271
  51.3 16.9 %collective-permute-start.6 = (bf16[96,2048]{1,0:T(8,128)(2,1)S(1)}, bf16[96,2048]{1,0:T(8,128)(2,1)S(1)}, u32[]{:S(2)}, u32[]{:S(2)}) collective-permute-start(bf16[96,2048]{1,0:T(8,128)(2,1)S(1)} %reshape.76.refs_0_), channel_id=1, source_target_pairs={{0,2},{1,3},{2,0},{3,1},{4,6},{5,7},{6,4},{7,5},{8,10},{9,11},{10,... | collective-permute-start | bytes 1179656 | tf_op jit(solution)/shard_map/ppermute | solution.py:271
  53.7 36.9 %all-to-all-start.2 = ((bf16[32,48,128]{2,1,0:T(8,128)(2,1)}), bf16[32,48,128]{2,1,0:T(8,128)(2,1)}, u32[]{:S(2)}, u32[]{:S(2)}) async-start(bf16[32,48,128]{2,1,0:T(8,128)(2,1)} %reshape.79), calls=%async_computation.3 | async-start | bytes 786432 | tf_op jit(solution)/shard_map/all_to_all | solution.py:349
  68.2 0.7 copy-start.11
  69.0 2.0 %copy-start.3 = (bf16[1,2048,896]{2,1,0:T(8,128)(2,1)S(1)}, bf16[1,2048,896]{2,1,0:T(8,128)(2,1)}, u32[]{:S(2)}) copy-start(bf16[1,2048,896]{2,1,0:T(8,128)(2,1)} %param.31) | copy-start | bytes 11010052
  71.0 2.0 %copy-start.5 = (bf16[1,2048,896]{2,1,0:T(8,128)(2,1)S(1)}, bf16[1,2048,896]{2,1,0:T(8,128)(2,1)}, u32[]{:S(2)}) copy-start(bf16[1,2048,896]{2,1,0:T(8,128)(2,1)} %param.32) | copy-start | bytes 11010052
  73.1 2.0 %copy-start.7 = (bf16[1,896,2048]{2,1,0:T(8,128)(2,1)S(1)}, bf16[1,896,2048]{2,1,0:T(8,128)(2,1)}, u32[]{:S(2)}) copy-start(bf16[1,896,2048]{2,1,0:T(8,128)(2,1)} %param.33) | copy-start | bytes 11010052
  75.1 1.0 copy-start.12
  81.2 13.7 %collective-permute-start.9 = (bf16[96,2048]{1,0:T(8,128)(2,1)S(1)}, bf16[96,2048]{1,0:T(8,128)(2,1)}, u32[]{:S(2)}, u32[]{:S(2)}) collective-permute-start(bf16[96,2048]{1,0:T(8,128)(2,1)S(1)} %get-tuple-element.22), channel_id=1, source_target_pairs={{0,2},{1,3},{2,0},{3,1},{4,6},{5,7},{6,4},{7,5},{8,10},{9,11},{10,... | collective-permute-start | bytes 1179656 | tf_op jit(solution)/shard_map/ppermute | solution.py:271
  83.2 18.8 %collective-permute-start.8 = (bf16[96,2048]{1,0:T(8,128)(2,1)S(1)}, bf16[96,2048]{1,0:T(8,128)(2,1)}, u32[]{:S(2)}, u32[]{:S(2)}) collective-permute-start(bf16[96,2048]{1,0:T(8,128)(2,1)S(1)} %get-tuple-element.21), channel_id=1, source_target_pairs={{0,1},{1,2},{2,3},{3,0},{4,5},{5,6},{6,7},{7,4},{8,9},{9,10},{10,1... | collective-permute-start | bytes 1179656 | tf_op jit(solution)/shard_map/ppermute | solution.py:271
  83.4 18.6 %collective-permute-start.7 = (bf16[96,2048]{1,0:T(8,128)(2,1)S(1)}, bf16[96,2048]{1,0:T(8,128)(2,1)}, u32[]{:S(2)}, u32[]{:S(2)}) collective-permute-start(bf16[96,2048]{1,0:T(8,128)(2,1)S(1)} %get-tuple-element.20), channel_id=1, source_target_pairs={{0,3},{1,0},{2,1},{3,2},{4,7},{5,4},{6,5},{7,6},{8,11},{9,8},{10,9... | collective-permute-start | bytes 1179656 | tf_op jit(solution)/shard_map/ppermute | solution.py:271
  85.2 1.4 collective-permute-start
  87.3 45.8 %collective-permute-start.1 = (bf16[1536,128]{1,0:T(8,128)(2,1)}, bf16[1536,128]{1,0:T(8,128)(2,1)}, u32[]{:S(2)}, u32[]{:S(2)}) collective-permute-start(bf16[1536,128]{1,0:T(8,128)(2,1)} %constant_dynamic-update-slice_fusion.refs_0_), channel_id=1, source_target_pairs={{0,8},{8,16},{16,24},{24,0},{1,9},{9,17},{17,25},{25,1},{2,10},{10... | collective-permute-start | bytes 1179656 | tf_op jit(solution)/shard_map/ppermute | solution.py:271
  88.9 46.3 %collective-permute-start.2 = (bf16[1536,128]{1,0:T(8,128)(2,1)}, bf16[1536,128]{1,0:T(8,128)(2,1)}, u32[]{:S(2)}, u32[]{:S(2)}) collective-permute-start(bf16[1536,128]{1,0:T(8,128)(2,1)} %constant_dynamic-update-slice_fusion.refs_0_), channel_id=1, source_target_pairs={{0,24},{8,0},{16,8},{24,16},{1,25},{9,1},{17,9},{25,17},{2,26},{10... | collective-permute-start | bytes 1179656 | tf_op jit(solution)/shard_map/ppermute | solution.py:271
  94.9 16.2 %collective-permute-start.11 = (bf16[96,2048]{1,0:T(8,128)(2,1)S(1)}, bf16[96,2048]{1,0:T(8,128)(2,1)S(1)}, u32[]{:S(2)}, u32[]{:S(2)}) collective-permute-start(bf16[96,2048]{1,0:T(8,128)(2,1)S(1)} %reshape.80.refs_0_), channel_id=1, source_target_pairs={{0,1},{1,2},{2,3},{3,0},{4,5},{5,6},{6,7},{7,4},{8,9},{9,10},{10,1... | collective-permute-start | bytes 1179656 | tf_op jit(solution)/shard_map/ppermute | solution.py:271
  101.9 12.5 %collective-permute-start.12 = (bf16[96,2048]{1,0:T(8,128)(2,1)S(1)}, bf16[96,2048]{1,0:T(8,128)(2,1)S(1)}, u32[]{:S(2)}, u32[]{:S(2)}) collective-permute-start(bf16[96,2048]{1,0:T(8,128)(2,1)S(1)} %reshape.80.refs_0_), channel_id=1, source_target_pairs={{0,3},{1,0},{2,1},{3,2},{4,7},{5,4},{6,5},{7,6},{8,11},{9,8},{10,9... | collective-permute-start | bytes 1179656 | tf_op jit(solution)/shard_map/ppermute | solution.py:271
  101.9 17.9 %collective-permute-start.13 = (bf16[96,2048]{1,0:T(8,128)(2,1)S(1)}, bf16[96,2048]{1,0:T(8,128)(2,1)S(1)}, u32[]{:S(2)}, u32[]{:S(2)}) collective-permute-start(bf16[96,2048]{1,0:T(8,128)(2,1)S(1)} %reshape.80.refs_0_), channel_id=1, source_target_pairs={{0,2},{1,3},{2,0},{3,1},{4,6},{5,7},{6,4},{7,5},{8,10},{9,11},{10,... | collective-permute-start | bytes 1179656 | tf_op jit(solution)/shard_map/ppermute | solution.py:271
  105.7 47.6 %all-to-all-start.1 = ((bf16[32,48,128]{2,1,0:T(8,128)(2,1)}), bf16[32,48,128]{2,1,0:T(8,128)(2,1)}, u32[]{:S(2)}, u32[]{:S(2)}) async-start(bf16[32,48,128]{2,1,0:T(8,128)(2,1)} %reshape.77), calls=%async_computation.2 | async-start | bytes 786432 | tf_op jit(solution)/shard_map/all_to_all | solution.py:349
  111.0 74.2 %reduce-scatter.2.cloned.1.call-start = ((), (), s32[]{:S(2)}) async-start(), calls=%async_computation.6 | async-start | bytes 1216512 | tf_op jit(solution)/shard_map/reduce_scatter | solution.py:422
  111.1 24.0 %collective-permute-start.3 = (bf16[1536,128]{1,0:T(8,128)(2,1)}, bf16[1536,128]{1,0:T(8,128)(2,1)}, u32[]{:S(2)}, u32[]{:S(2)}) collective-permute-start(bf16[1536,128]{1,0:T(8,128)(2,1)} %constant_dynamic-update-slice_fusion.refs_0_), channel_id=1, source_target_pairs={{0,16},{8,24},{16,0},{24,8},{1,17},{9,25},{17,1},{25,9},{2,18},{10... | collective-permute-start | bytes 1179656 | tf_op jit(solution)/shard_map/ppermute | solution.py:271
  119.8 0.8 copy-start.9
  120.6 2.0 %copy-start.4 = (bf16[1,2048,896]{2,1,0:T(8,128)(2,1)S(1)}, bf16[1,2048,896]{2,1,0:T(8,128)(2,1)}, u32[]{:S(2)}) copy-start(bf16[1,2048,896]{2,1,0:T(8,128)(2,1)} %param.31) | copy-start | bytes 11010052
  122.6 2.0 %copy-start.6 = (bf16[1,2048,896]{2,1,0:T(8,128)(2,1)S(1)}, bf16[1,2048,896]{2,1,0:T(8,128)(2,1)}, u32[]{:S(2)}) copy-start(bf16[1,2048,896]{2,1,0:T(8,128)(2,1)} %param.32) | copy-start | bytes 11010052
  124.6 2.0 %copy-start.8 = (bf16[1,896,2048]{2,1,0:T(8,128)(2,1)S(1)}, bf16[1,896,2048]{2,1,0:T(8,128)(2,1)}, u32[]{:S(2)}) copy-start(bf16[1,896,2048]{2,1,0:T(8,128)(2,1)} %param.33) | copy-start | bytes 11010052
  126.7 1.0 copy-start.10
  132.8 17.8 %collective-permute-start.16 = (bf16[96,2048]{1,0:T(8,128)(2,1)S(1)}, bf16[96,2048]{1,0:T(8,128)(2,1)S(1)}, u32[]{:S(2)}, u32[]{:S(2)}) collective-permute-start(bf16[96,2048]{1,0:T(8,128)(2,1)S(1)} %get-tuple-element.27), channel_id=1, source_target_pairs={{0,2},{1,3},{2,0},{3,1},{4,6},{5,7},{6,4},{7,5},{8,10},{9,11},{10,... | collective-permute-start | bytes 1179656 | tf_op jit(solution)/shard_map/ppermute | solution.py:271
  133.1 17.5 %collective-permute-start.15 = (bf16[96,2048]{1,0:T(8,128)(2,1)S(1)}, bf16[96,2048]{1,0:T(8,128)(2,1)S(1)}, u32[]{:S(2)}, u32[]{:S(2)}) collective-permute-start(bf16[96,2048]{1,0:T(8,128)(2,1)S(1)} %get-tuple-element.26), channel_id=1, source_target_pairs={{0,1},{1,2},{2,3},{3,0},{4,5},{5,6},{6,7},{7,4},{8,9},{9,10},{10,1... | collective-permute-start | bytes 1179656 | tf_op jit(solution)/shard_map/ppermute | solution.py:271
  133.1 19.1 %collective-permute-start.14 = (bf16[96,2048]{1,0:T(8,128)(2,1)S(1)}, bf16[96,2048]{1,0:T(8,128)(2,1)S(1)}, u32[]{:S(2)}, u32[]{:S(2)}) collective-permute-start(bf16[96,2048]{1,0:T(8,128)(2,1)S(1)} %get-tuple-element.25), channel_id=1, source_target_pairs={{0,3},{1,0},{2,1},{3,2},{4,7},{5,4},{6,5},{7,6},{8,11},{9,8},{10,9... | collective-permute-start | bytes 1179656 | tf_op jit(solution)/shard_map/ppermute | solution.py:271
  153.3 31.9 %copy-start.2 = (f32[128]{0:T(128)S(1)}, f32[128]{0:T(128)}, u32[]{:S(2)}) copy-start(f32[128]{0:T(128)} %param.26) | copy-start | bytes 1540
  153.3 22.5 %all-to-all-start.3 = ((bf16[32,48,128]{2,1,0:T(8,128)(2,1)}), bf16[32,48,128]{2,1,0:T(8,128)(2,1)S(1)}, u32[]{:S(2)}, u32[]{:S(2)}) async-start(bf16[32,48,128]{2,1,0:T(8,128)(2,1)} %reshape.81), calls=%async_computation.4 | async-start | bytes 786432 | tf_op jit(solution)/shard_map/all_to_all | solution.py:349
  176.0 1.8 collective-permute-start.17
  185.2 0.9 copy-start.1
Sparse Core Ops, SparseCore 0:
  13.0 57.8 all-gather.1
  150.7 34.4 reduce-scatter.1
where the time goes:
time: 195 us; the launch traced here: 194 us
  waiting for transfers between devices  68 us (35%)
  starting transfers between devices  47.8 us (25%)
  Pallas kernels  31.6 us (16%)
  local copies, waits for them, and re-layouts  27.6 us (14%)
  between operations  14.3 us (7%)
  other arithmetic  3 us (2%)
    all_to_all x4, waiting for transfers between devices, dispatch(): return lax.all_to_all(blocks, ZY, 0, 0, tiled=True).reshape(rows.shape)  33.9 us
    all_to_all x4, starting transfers between devices, dispatch(): return lax.all_to_all(blocks, ZY, 0, 0, tiled=True).reshape(rows.shape)  28.4 us
    ppermute x18, waiting for transfers between devices, shifted(): return lax.ppermute(x, axis, [(i, (i + by) % count) for i in range(count)])  27.8 us
    unnamed x29, local copies, waits for them, and re-layouts  20.3 us
    ppermute x18, starting transfers between devices, shifted(): return lax.ppermute(x, axis, [(i, (i + by) % count) for i in range(count)])  19.3 us
    pallas_call x1, Pallas kernels, flash(): pl.pallas_call(functools.partial(flash_body, groups, rows, scale, len(pie...  15.4 us
    pallas_call x2, Pallas kernels, mlp(): pl.pallas_call(functools.partial(mlp_body, len(xs)), in_specs=[whole] * (...  10.2 us
    reduce_scatter x1, waiting for transfers between devices, on_device(): parts = lax.psum_scatter(parts, YC, scatter_dimension=0, tiled=True)  6.26 us
  transfers between devices with their start and end apart: 24, of which 11 were waited for; matrix products, arithmetic and copies ran while one was open for 7% of the time, Pallas kernels for 13%

commit v1 on v0

--- a/solution.py
+++ b/solution.py
@@ -276,7 +276,12 @@
     rows = tokens_ref.shape[0]
     lane = lax.broadcasted_iota(jnp.int32, (rows, 128), 1)
     normed = rms_norm(tokens_ref[...].astype(jnp.float32), gain_ref[...]).astype(jnp.bfloat16)
-    chosen = [routes_ref[:, k : k + 1] for k in range(2)]
+    place = lax.broadcasted_iota(jnp.int32, (rows, routes_ref.shape[1]), 0) + at_ref[0] * rows
+    own = place == lax.broadcasted_iota(jnp.int32, place.shape, 1)
+    names = routes_ref[...].astype(jnp.float32)
+    chosen = [
+        jnp.sum(jnp.where(own, names[k : k + 1, :], 0.0), axis=1, keepdims=True).astype(jnp.int32) for k in range(2)
+    ]
     named = [(c == lane).astype(jnp.float32) for c in chosen]
     before = lax.broadcasted_iota(jnp.int32, (rows, rows), 1) < lax.broadcasted_iota(jnp.int32, (rows, rows), 0)
     count = jnp.dot(
@@ -307,7 +312,7 @@
         num_scalar_prefetch=1,
         grid=(1,),
         in_specs=[
-            pl.BlockSpec((part_rows, 2), lambda s, i: (i[0], 0)),
+            pl.BlockSpec((2, moe_tokens.shape[0]), lambda s, i: (0, 0)),
             pl.BlockSpec((part_rows, dim), lambda s, i: (i[0], 0)),
             pl.BlockSpec((1, dim), lambda s, i: (0, 0)),
         ],
@@ -327,7 +332,7 @@
         ],
         compiler_params=pltpu.CompilerParams(vmem_limit_bytes=16 << 20),
         name="send",
-    )(at, in_hbm(routes), in_hbm(moe_tokens), in_hbm(moe_gain.reshape(1, -1)))
+    )(at, in_hbm(routes.T), in_hbm(moe_tokens), in_hbm(moe_gain.reshape(1, -1)))
 
 
 def experts_part(moe_tokens, moe_gain, routes, route_weights, w_gate, w_up, w_down, queries, attend):
@@ -367,8 +372,11 @@
     parts = attend(queries)
     near_sum = total(near_y)
     far_sum = total(far_y)
-    near_back = dispatch(near_sum)
-    far_back = dispatch(far_sum)
+    both = jnp.concatenate([s.reshape(zy_count, -1, 128) for s in (near_sum, far_sum)], axis=1)
+    both = lax.all_to_all(both, ZY, 0, 0, tiled=True)
+    cut = both.shape[1] // 2
+    near_back = both[:, :cut].reshape(near_sum.shape)
+    far_back = both[:, cut:].reshape(far_sum.shape)
     far_back = shifted(far_back, CORE, 1)
     mixed = jnp.zeros((part_rows, near_back.shape[1]), jnp.float32)
     for k in range(top_count):
@@ -407,8 +415,8 @@
             raw_queries, kv_latent, rope_key, latent_gain, w_key_up, w_value_up, query_gain, key_gain, rope_gain, positions
         )
         keys = lax.all_gather(keys, "ep_0", axis=0, tiled=True)
+        shifts = (0, 1, 3, 2)
         pair = jnp.concatenate([own, shifted(own, CORE, 1)], axis=0)
-        shifts = (0, 1, 3, 2)
         pieces = [pair] + [shifted(pair, "ep_1", s) for s in shifts[1:]]
         row = lax.axis_index("ep_1")
         core = lax.axis_index(CORE)

time: 195 us -> 196 us (level)
  the two profiles are of different devices: /device:TPU:6 before, /device:TPU:2 now
where the time goes in v1:
time: 196 us; the launch traced here: 195 us
  waiting for transfers between devices  71.7 us (37%)
  starting transfers between devices  58.3 us (30%)
  Pallas kernels  31.4 us (16%)
  between operations  14.3 us (7%)
  local copies, waits for them, and re-layouts  13.9 us (7%)
  other arithmetic  3.79 us (2%)
    ppermute x18, starting transfers between devices, shifted(): return lax.ppermute(x, axis, [(i, (i + by) % count) for i in range(count)])  33.8 us
    reduce_scatter x1, waiting for transfers between devices, on_device(): parts = lax.psum_scatter(parts, YC, scatter_dimension=0, tiled=True)  26.8 us
    all_to_all x2, waiting for transfers between devices, dispatch(): return lax.all_to_all(blocks, ZY, 0, 0, tiled=True).reshape(rows.shape)  26.7 us
    all_to_all x2, starting transfers between devices, dispatch(): return lax.all_to_all(blocks, ZY, 0, 0, tiled=True).reshape(rows.shape)  15.4 us
    pallas_call x1, Pallas kernels, flash(): pl.pallas_call(functools.partial(flash_body, groups, rows, scale, len(pie...  15.4 us
    ppermute x18, waiting for transfers between devices, shifted(): return lax.ppermute(x, axis, [(i, (i + by) % count) for i in range(count)])  12.9 us
    pallas_call x2, Pallas kernels, mlp(): pl.pallas_call(functools.partial(mlp_body, len(xs)), in_specs=[whole] * (...  10.1 us
    unnamed x18, local copies, waits for them, and re-layouts  9.96 us
  transfers between devices with their start and end apart: 23, of which 11 were waited for; matrix products, arithmetic and copies ran while one was open for 4% of the time, Pallas kernels for 13%

profile of v1, /device:TPU:2, one launch (start us, length us, event | category | flops | bytes accessed | tf_op | source)
XLA Modules:
  0.0 195.0 jit_solution(5477341572740930900)
XLA Ops:
  7.3 1.5 copy.19.refs_2_
  8.8 0.1 mul.83
  8.8 1.2 fusion.4
  10.1 2.8 %prepare.1 = (bf16[1152,128]{1,0:T(8,128)(2,1)}, bf16[768,128]{1,0:T(8,128)(2,1)S(1)}) custom-call(bf16[256,384]{1,0:T(8,128)(2,1)} %refs_0_.1, bf16[256,512]{1,0:T(8,128)(2,1)} %refs_1_.1, bf16[256,64]{1,0:T(8,128)(2,1)} %copy.19.refs_2_, f32[1,512]{1,0:T(1,128)} %bitcast.50, bf16[512,256]{1,0:T(8,128)(2,1)} %refs_4_.1, bf16[512,256]{1,0:T(8,128)(2,1)} %refs_5_.1, ...), custom_call_target="tpu_custom_call" | custom-call | flops 134217728 | bytes 2097152 | tf_op jit(solution)/shard_map/prepare/pallas_call | solution.py:86
  13.0 2.3 %send.1 = (bf16[96,2048]{1,0:T(8,128)(2,1)S(1)}, bf16[96,2048]{1,0:T(8,128)(2,1)S(1)}, bf16[2,2,64,128]{3,2,1,0:T(8,128)(2,1)S(1)}) custom-call(s32[2]{0:T(128)S(1)} %pad_add_fusion.at_ref, s32[2,256]{1,0:T(2,128)} %bitcast.51, bf16[256,2048]{1,0:T(8,128)(2,1)} %tokens_ref.1, f32[1,2048]{1,0:T(1,128)} %bitcast.49), custom_call_target="tpu_custom_call" | custom-call | tf_op jit(solution)/shard_map/send/pallas_call | solution.py:325
  15.2 1.0 reshape.75
  16.2 11.5 %all-to-all-start = ((bf16[32,48,128]{2,1,0:T(8,128)(2,1)}), bf16[32,48,128]{2,1,0:T(8,128)(2,1)S(1)}, u32[]{:S(2)}, u32[]{:S(2)}) async-start(bf16[32,48,128]{2,1,0:T(8,128)(2,1)} %reshape.75), calls=%async_computation.1 | async-start | bytes 786432 | tf_op jit(solution)/shard_map/all_to_all | solution.py:354
  27.7 0.1 collective-permute-start.10
  27.8 1.7 collective-permute-done.10
  29.5 0.9 reshape.78
  30.4 17.2 %all-to-all-done = bf16[32,48,128]{2,1,0:T(8,128)(2,1)S(1)} async-done(((bf16[32,48,128]{2,1,0:T(8,128)(2,1)}), bf16[32,48,128]{2,1,0:T(8,128)(2,1)S(1)}, u32[]{:S(2)}, u32[]{:S(2)}) %all-to-all-start) | async-done | bytes 393248 | tf_op jit(solution)/shard_map/all_to_all | solution.py:354
  47.7 4.0 %all-to-all-start.1 = ((bf16[32,48,128]{2,1,0:T(8,128)(2,1)}), bf16[32,48,128]{2,1,0:T(8,128)(2,1)S(1)}, u32[]{:S(2)}, u32[]{:S(2)}) async-start(bf16[32,48,128]{2,1,0:T(8,128)(2,1)} %reshape.78), calls=%async_computation.2 | async-start | bytes 786432 | tf_op jit(solution)/shard_map/all_to_all | solution.py:354
  51.6 0.2 reshape.76.refs_0_
  51.8 1.6 collective-permute-start.4
  53.4 0.5 collective-permute-start.5
  53.9 2.1 %collective-permute-start.6 = (bf16[96,2048]{1,0:T(8,128)(2,1)S(1)}, bf16[96,2048]{1,0:T(8,128)(2,1)S(1)}, u32[]{:S(2)}, u32[]{:S(2)}) collective-permute-start(bf16[96,2048]{1,0:T(8,128)(2,1)S(1)} %reshape.76.refs_0_), channel_id=1, source_target_pairs={{0,2},{1,3},{2,0},{3,1},{4,6},{5,7},{6,4},{7,5},{8,10},{9,11},{10,... | collective-permute-start | bytes 1179656 | tf_op jit(solution)/shard_map/ppermute | solution.py:271
  56.0 0.1 stack.52.at_ref
  56.1 0.7 constant_dynamic-update-slice_fusion.1
  56.8 0.6 collective-permute-done
  57.5 0.7 constant_dynamic-update-slice_fusion.refs_0_
  58.2 1.8 collective-permute-start.1
  60.0 1.4 collective-permute-start.2
  61.4 9.5 %all-to-all-done.1 = bf16[32,48,128]{2,1,0:T(8,128)(2,1)S(1)} async-done(((bf16[32,48,128]{2,1,0:T(8,128)(2,1)}), bf16[32,48,128]{2,1,0:T(8,128)(2,1)S(1)}, u32[]{:S(2)}, u32[]{:S(2)}) %all-to-all-start.1) | async-done | bytes 393248 | tf_op jit(solution)/shard_map/all_to_all | solution.py:354
  70.9 0.2 reshape.79.refs_0_
  71.1 1.6 collective-permute-start.11
  72.7 0.5 collective-permute-start.12
  73.2 2.2 %collective-permute-start.13 = (bf16[96,2048]{1,0:T(8,128)(2,1)S(1)}, bf16[96,2048]{1,0:T(8,128)(2,1)S(1)}, u32[]{:S(2)}, u32[]{:S(2)}) collective-permute-start(bf16[96,2048]{1,0:T(8,128)(2,1)S(1)} %reshape.79.refs_0_), channel_id=1, source_target_pairs={{0,2},{1,3},{2,0},{3,1},{4,6},{5,7},{6,4},{7,5},{8,10},{9,11},{10,... | collective-permute-start | bytes 1179656 | tf_op jit(solution)/shard_map/ppermute | solution.py:271
  75.4 2.0 %copy-done.3 = bf16[1,2048,896]{2,1,0:T(8,128)(2,1)S(1)} copy-done((bf16[1,2048,896]{2,1,0:T(8,128)(2,1)S(1)}, bf16[1,2048,896]{2,1,0:T(8,128)(2,1)}, u32[]{:S(2)}) %copy-start.3) | copy-done | bytes 3670040
  77.4 2.0 %copy-done.5 = bf16[1,2048,896]{2,1,0:T(8,128)(2,1)S(1)} copy-done((bf16[1,2048,896]{2,1,0:T(8,128)(2,1)S(1)}, bf16[1,2048,896]{2,1,0:T(8,128)(2,1)}, u32[]{:S(2)}) %copy-start.5) | copy-done | bytes 3670040
  79.5 2.0 %copy-done.6 = bf16[1,896,2048]{2,1,0:T(8,128)(2,1)S(1)} copy-done((bf16[1,896,2048]{2,1,0:T(8,128)(2,1)S(1)}, bf16[1,896,2048]{2,1,0:T(8,128)(2,1)}, u32[]{:S(2)}) %copy-start.6) | copy-done | bytes 3670040
  81.5 5.1 %mlp.2 = (f32[96,2048]{1,0:T(8,128)S(1)}, bf16[96,2048]{1,0:T(8,128)(2,1)S(1)}, bf16[96,2048]{1,0:T(8,128)(2,1)S(1)}, bf16[96,2048]{1,0:T(8,128)(2,1)S(1)}) custom-call(bf16[96,2048]{1,0:T(8,128)(2,1)S(1)} %reshape.76.refs_0_, bf16[96,2048]{1,0:T(8,128)(2,1)S(1)} %collective-permute-done.4.refs_1_, bf16[96,2048]{1,0:T(8,128)(2,1)S(1)} %collective-permute-done.5.refs_2_, ...), custom_call_target="tpu_custom_call" | custom-call | flops 4227858432 | bytes 11010048 | tf_op jit(solution)/shard_map/mlp/pallas_call | solution.py:256
  86.6 1.5 collective-permute-start.9
  88.1 4.9 %collective-permute-start.8 = (bf16[96,2048]{1,0:T(8,128)(2,1)S(1)}, bf16[96,2048]{1,0:T(8,128)(2,1)S(1)}, u32[]{:S(2)}, u32[]{:S(2)}) collective-permute-start(bf16[96,2048]{1,0:T(8,128)(2,1)S(1)} %get-tuple-element.21), channel_id=1, source_target_pairs={{0,1},{1,2},{2,3},{3,0},{4,5},{5,6},{6,7},{7,4},{8,9},{9,10},{10,1... | collective-permute-start | bytes 1179656 | tf_op jit(solution)/shard_map/ppermute | solution.py:271
  92.9 2.1 %collective-permute-start.7 = (bf16[96,2048]{1,0:T(8,128)(2,1)S(1)}, bf16[96,2048]{1,0:T(8,128)(2,1)S(1)}, u32[]{:S(2)}, u32[]{:S(2)}) collective-permute-start(bf16[96,2048]{1,0:T(8,128)(2,1)S(1)} %get-tuple-element.20), channel_id=1, source_target_pairs={{0,3},{1,0},{2,1},{3,2},{4,7},{5,4},{6,5},{7,6},{8,11},{9,8},{10,9... | collective-permute-start | bytes 1179656 | tf_op jit(solution)/shard_map/ppermute | solution.py:271
  95.1 5.0 %mlp.3 = (f32[96,2048]{1,0:T(8,128)S(1)}, bf16[96,2048]{1,0:T(8,128)(2,1)S(1)}, bf16[96,2048]{1,0:T(8,128)(2,1)S(1)}, bf16[96,2048]{1,0:T(8,128)(2,1)S(1)}) custom-call(bf16[96,2048]{1,0:T(8,128)(2,1)S(1)} %reshape.79.refs_0_, bf16[96,2048]{1,0:T(8,128)(2,1)S(1)} %collective-permute-done.11.refs_1_, bf16[96,2048]{1,0:T(8,128)(2,1)S(1)} %collective-permute-done.12.refs_2_, ...), custom_call_target="tpu_custom_call" | custom-call | flops 4227858432 | bytes 11010048 | tf_op jit(solution)/shard_map/mlp/pallas_call | solution.py:256
  100.2 4.4 %collective-permute-start.16 = (bf16[96,2048]{1,0:T(8,128)(2,1)S(1)}, bf16[96,2048]{1,0:T(8,128)(2,1)S(1)}, u32[]{:S(2)}, u32[]{:S(2)}) collective-permute-start(bf16[96,2048]{1,0:T(8,128)(2,1)S(1)} %get-tuple-element.27), channel_id=1, source_target_pairs={{0,2},{1,3},{2,0},{3,1},{4,6},{5,7},{6,4},{7,5},{8,10},{9,11},{10,... | collective-permute-start | bytes 1179656 | tf_op jit(solution)/shard_map/ppermute | solution.py:271
  104.6 5.7 %collective-permute-done.8 = bf16[96,2048]{1,0:T(8,128)(2,1)S(1)} collective-permute-done((bf16[96,2048]{1,0:T(8,128)(2,1)S(1)}, bf16[96,2048]{1,0:T(8,128)(2,1)S(1)}, u32[]{:S(2)}, u32[]{:S(2)}) %collective-permute-start.8) | collective-permute-done | bytes 393248 | tf_op jit(solution)/shard_map/ppermute | solution.py:271
  110.3 0.3 collective-permute-start.15
  110.6 0.9 collective-permute-done.7
  111.5 5.8 %collective-permute-start.14 = (bf16[96,2048]{1,0:T(8,128)(2,1)S(1)}, bf16[96,2048]{1,0:T(8,128)(2,1)}, u32[]{:S(2)}, u32[]{:S(2)}) collective-permute-start(bf16[96,2048]{1,0:T(8,128)(2,1)S(1)} %get-tuple-element.25), channel_id=1, source_target_pairs={{0,3},{1,0},{2,1},{3,2},{4,7},{5,4},{6,5},{7,6},{8,11},{9,8},{10,9... | collective-permute-start | bytes 1179656 | tf_op jit(solution)/shard_map/ppermute | solution.py:271
  117.3 0.2 add_convert_fusion.1
  117.5 0.2 reshape.77
  117.7 0.2 collective-permute-done.16
  117.9 2.9 %collective-permute-start.3 = (bf16[1536,128]{1,0:T(8,128)(2,1)}, bf16[1536,128]{1,0:T(8,128)(2,1)S(1)}, u32[]{:S(2)}, u32[]{:S(2)}) collective-permute-start(bf16[1536,128]{1,0:T(8,128)(2,1)} %constant_dynamic-update-slice_fusion.refs_0_), channel_id=1, source_target_pairs={{0,16},{8,24},{16,0},{24,8},{1,17},{9,25},{17,1},{25,9},{2,18},{10... | collective-permute-start | bytes 1179656 | tf_op jit(solution)/shard_map/ppermute | solution.py:271
  120.8 2.4 %collective-permute-done.15 = bf16[96,2048]{1,0:T(8,128)(2,1)} collective-permute-done((bf16[96,2048]{1,0:T(8,128)(2,1)S(1)}, bf16[96,2048]{1,0:T(8,128)(2,1)}, u32[]{:S(2)}, u32[]{:S(2)}) %collective-permute-start.15) | collective-permute-done | bytes 393248 | tf_op jit(solution)/shard_map/ppermute | solution.py:271
  123.2 1.3 add_convert_fusion
  124.5 0.2 reshape.80
  124.7 0.9 pad_maximum_fusion
  125.6 8.7 %all-to-all-start.2 = ((bf16[32,96,128]{2,1,0:T(8,128)(2,1)}), bf16[32,96,128]{2,1,0:T(8,128)(2,1)S(1)}, u32[]{:S(2)}, u32[]{:S(2)}) async-start(bf16[32,96,128]{2,1,0:T(8,128)(2,1)} %pad_maximum_fusion), calls=%async_computation.3 | async-start | bytes 1572864 | tf_op jit(solution)/shard_map/all_to_all | solution.py:376
  134.3 0.3 reduce-scatter.2.cloned.1.call-start
  134.7 0.7 copy-done.7
  135.4 15.4 %flash.1 = bf16[4224,128]{1,0:T(8,128)(2,1)} custom-call(s32[10]{0:T(128)S(1)} %stack.52.at_ref, bf16[1536,128]{1,0:T(8,128)(2,1)} %constant_dynamic-update-slice_fusion.refs_0_, bf16[1536,128]{1,0:T(8,128)(2,1)} %collective-permute-done.1.refs_1_, bf16[1536,128]{1,0:T(8,128)(2,1)} %collective-permute-done.2.refs_2_, bf16[1536,128]{1,0:T(8,128)(2,1)} %copy-done.7, ...), custom_call_target="tpu_custom_call" | custom-call | flops 8589934592 | bytes 4194304 | tf_op jit(solution)/shard_map/flash/pallas_call | solution.py:195
  150.9 5.2 %all-to-all-done.2 = bf16[32,96,128]{2,1,0:T(8,128)(2,1)S(1)} async-done(((bf16[32,96,128]{2,1,0:T(8,128)(2,1)}), bf16[32,96,128]{2,1,0:T(8,128)(2,1)S(1)}, u32[]{:S(2)}, u32[]{:S(2)}) %all-to-all-start.2) | async-done | bytes 786464 | tf_op jit(solution)/shard_map/all_to_all | solution.py:376
  156.2 0.2 reshape.81
  156.4 0.2 reshape.82
  156.5 0.1 collective-permute-start.17
  156.7 0.2 fusion.9
  156.9 0.2 fusion.6
  157.1 1.3 collective-permute-done.17
  158.4 0.2 fusion.2
  158.6 0.9 fusion.3
  159.5 26.8 %reduce-scatter.2.cloned.1.call-done.in_ref = bf16[528,128]{1,0:T(8,128)(2,1)} async-done(((bf16[4224,128]{1,0:T(8,128)(2,1)}), bf16[528,128]{1,0:T(8,128)(2,1)}) %reduce-scatter.2.cloned.1.call-update) | async-done | bytes 135184 | tf_op jit(solution)/shard_map/reduce_scatter | solution.py:430
  186.3 0.9 copy-done.1
  187.2 0.9 finish.1
  (35 shorter events, 0.4 us)
Async XLA Ops:
  7.2 143.7 %copy-start = (f32[256,2]{0,1:T(2,128)S(1)}, f32[256,2]{0,1:T(2,128)}, u32[]{:S(2)}) copy-start(f32[256,2]{0,1:T(2,128)} %param.30) | copy-start | bytes 6148
  7.2 127.5 %all-gather.2.cloned.1.call-start = ((), (), s32[]{:S(2)}) async-start(), calls=%async_computation.4 | async-start | bytes 2654208 | tf_op jit(solution)/shard_map/all_gather | solution.py:417
  16.2 31.5 %all-to-all-start = ((bf16[32,48,128]{2,1,0:T(8,128)(2,1)}), bf16[32,48,128]{2,1,0:T(8,128)(2,1)S(1)}, u32[]{:S(2)}, u32[]{:S(2)}) async-start(bf16[32,48,128]{2,1,0:T(8,128)(2,1)} %reshape.75), calls=%async_computation.1 | async-start | bytes 786432 | tf_op jit(solution)/shard_map/all_to_all | solution.py:354
  27.7 1.8 collective-permute-start.10
  47.7 23.3 %all-to-all-start.1 = ((bf16[32,48,128]{2,1,0:T(8,128)(2,1)}), bf16[32,48,128]{2,1,0:T(8,128)(2,1)S(1)}, u32[]{:S(2)}, u32[]{:S(2)}) async-start(bf16[32,48,128]{2,1,0:T(8,128)(2,1)} %reshape.78), calls=%async_computation.2 | async-start | bytes 786432 | tf_op jit(solution)/shard_map/all_to_all | solution.py:354
  51.8 19.3 %collective-permute-start.4 = (bf16[96,2048]{1,0:T(8,128)(2,1)S(1)}, bf16[96,2048]{1,0:T(8,128)(2,1)S(1)}, u32[]{:S(2)}, u32[]{:S(2)}) collective-permute-start(bf16[96,2048]{1,0:T(8,128)(2,1)S(1)} %reshape.76.refs_0_), channel_id=1, source_target_pairs={{0,1},{1,2},{2,3},{3,0},{4,5},{5,6},{6,7},{7,4},{8,9},{9,10},{10,1... | collective-permute-start | bytes 1179656 | tf_op jit(solution)/shard_map/ppermute | solution.py:271
  53.4 19.3 %collective-permute-start.5 = (bf16[96,2048]{1,0:T(8,128)(2,1)S(1)}, bf16[96,2048]{1,0:T(8,128)(2,1)S(1)}, u32[]{:S(2)}, u32[]{:S(2)}) collective-permute-start(bf16[96,2048]{1,0:T(8,128)(2,1)S(1)} %reshape.76.refs_0_), channel_id=1, source_target_pairs={{0,3},{1,0},{2,1},{3,2},{4,7},{5,4},{6,5},{7,6},{8,11},{9,8},{10,9... | collective-permute-start | bytes 1179656 | tf_op jit(solution)/shard_map/ppermute | solution.py:271
  53.9 19.3 %collective-permute-start.6 = (bf16[96,2048]{1,0:T(8,128)(2,1)S(1)}, bf16[96,2048]{1,0:T(8,128)(2,1)S(1)}, u32[]{:S(2)}, u32[]{:S(2)}) collective-permute-start(bf16[96,2048]{1,0:T(8,128)(2,1)S(1)} %reshape.76.refs_0_), channel_id=1, source_target_pairs={{0,2},{1,3},{2,0},{3,1},{4,6},{5,7},{6,4},{7,5},{8,10},{9,11},{10,... | collective-permute-start | bytes 1179656 | tf_op jit(solution)/shard_map/ppermute | solution.py:271
  56.0 1.4 collective-permute-start
  58.2 76.5 %collective-permute-start.1 = (bf16[1536,128]{1,0:T(8,128)(2,1)}, bf16[1536,128]{1,0:T(8,128)(2,1)}, u32[]{:S(2)}, u32[]{:S(2)}) collective-permute-start(bf16[1536,128]{1,0:T(8,128)(2,1)} %constant_dynamic-update-slice_fusion.refs_0_), channel_id=1, source_target_pairs={{0,8},{8,16},{16,24},{24,0},{1,9},{9,17},{17,25},{25,1},{2,10},{10... | collective-permute-start | bytes 1179656 | tf_op jit(solution)/shard_map/ppermute | solution.py:271
  60.0 74.7 %collective-permute-start.2 = (bf16[1536,128]{1,0:T(8,128)(2,1)}, bf16[1536,128]{1,0:T(8,128)(2,1)}, u32[]{:S(2)}, u32[]{:S(2)}) collective-permute-start(bf16[1536,128]{1,0:T(8,128)(2,1)} %constant_dynamic-update-slice_fusion.refs_0_), channel_id=1, source_target_pairs={{0,24},{8,0},{16,8},{24,16},{1,25},{9,1},{17,9},{25,17},{2,26},{10... | collective-permute-start | bytes 1179656 | tf_op jit(solution)/shard_map/ppermute | solution.py:271
  71.1 15.5 %collective-permute-start.11 = (bf16[96,2048]{1,0:T(8,128)(2,1)S(1)}, bf16[96,2048]{1,0:T(8,128)(2,1)S(1)}, u32[]{:S(2)}, u32[]{:S(2)}) collective-permute-start(bf16[96,2048]{1,0:T(8,128)(2,1)S(1)} %reshape.79.refs_0_), channel_id=1, source_target_pairs={{0,1},{1,2},{2,3},{3,0},{4,5},{5,6},{6,7},{7,4},{8,9},{9,10},{10,1... | collective-permute-start | bytes 1179656 | tf_op jit(solution)/shard_map/ppermute | solution.py:271
  72.7 15.4 %collective-permute-start.12 = (bf16[96,2048]{1,0:T(8,128)(2,1)S(1)}, bf16[96,2048]{1,0:T(8,128)(2,1)S(1)}, u32[]{:S(2)}, u32[]{:S(2)}) collective-permute-start(bf16[96,2048]{1,0:T(8,128)(2,1)S(1)} %reshape.79.refs_0_), channel_id=1, source_target_pairs={{0,3},{1,0},{2,1},{3,2},{4,7},{5,4},{6,5},{7,6},{8,11},{9,8},{10,9... | collective-permute-start | bytes 1179656 | tf_op jit(solution)/shard_map/ppermute | solution.py:271
  73.2 19.7 %collective-permute-start.13 = (bf16[96,2048]{1,0:T(8,128)(2,1)S(1)}, bf16[96,2048]{1,0:T(8,128)(2,1)S(1)}, u32[]{:S(2)}, u32[]{:S(2)}) collective-permute-start(bf16[96,2048]{1,0:T(8,128)(2,1)S(1)} %reshape.79.refs_0_), channel_id=1, source_target_pairs={{0,2},{1,3},{2,0},{3,1},{4,6},{5,7},{6,4},{7,5},{8,10},{9,11},{10,... | collective-permute-start | bytes 1179656 | tf_op jit(solution)/shard_map/ppermute | solution.py:271
  75.4 2.0 %copy-start.3 = (bf16[1,2048,896]{2,1,0:T(8,128)(2,1)S(1)}, bf16[1,2048,896]{2,1,0:T(8,128)(2,1)}, u32[]{:S(2)}) copy-start(bf16[1,2048,896]{2,1,0:T(8,128)(2,1)} %param.31) | copy-start | bytes 11010052
  77.4 2.0 %copy-start.5 = (bf16[1,2048,896]{2,1,0:T(8,128)(2,1)S(1)}, bf16[1,2048,896]{2,1,0:T(8,128)(2,1)}, u32[]{:S(2)}) copy-start(bf16[1,2048,896]{2,1,0:T(8,128)(2,1)} %param.32) | copy-start | bytes 11010052
  79.5 2.0 %copy-start.6 = (bf16[1,896,2048]{2,1,0:T(8,128)(2,1)S(1)}, bf16[1,896,2048]{2,1,0:T(8,128)(2,1)}, u32[]{:S(2)}) copy-start(bf16[1,896,2048]{2,1,0:T(8,128)(2,1)} %param.33) | copy-start | bytes 11010052
  81.5 13.6 %copy-start.4 = (bf16[1,2048,896]{2,1,0:T(8,128)(2,1)S(1)}, bf16[1,2048,896]{2,1,0:T(8,128)(2,1)}, u32[]{:S(2)}) copy-start(bf16[1,2048,896]{2,1,0:T(8,128)(2,1)} %param.31) | copy-start | bytes 11010052
  86.6 13.6 %collective-permute-start.9 = (bf16[96,2048]{1,0:T(8,128)(2,1)S(1)}, bf16[96,2048]{1,0:T(8,128)(2,1)S(1)}, u32[]{:S(2)}, u32[]{:S(2)}) collective-permute-start(bf16[96,2048]{1,0:T(8,128)(2,1)S(1)} %get-tuple-element.22), channel_id=1, source_target_pairs={{0,2},{1,3},{2,0},{3,1},{4,6},{5,7},{6,4},{7,5},{8,10},{9,11},{10,... | collective-permute-start | bytes 1179656 | tf_op jit(solution)/shard_map/ppermute | solution.py:271
  88.1 22.3 %collective-permute-start.8 = (bf16[96,2048]{1,0:T(8,128)(2,1)S(1)}, bf16[96,2048]{1,0:T(8,128)(2,1)S(1)}, u32[]{:S(2)}, u32[]{:S(2)}) collective-permute-start(bf16[96,2048]{1,0:T(8,128)(2,1)S(1)} %get-tuple-element.21), channel_id=1, source_target_pairs={{0,1},{1,2},{2,3},{3,0},{4,5},{5,6},{6,7},{7,4},{8,9},{9,10},{10,1... | collective-permute-start | bytes 1179656 | tf_op jit(solution)/shard_map/ppermute | solution.py:271
  92.9 18.6 %collective-permute-start.7 = (bf16[96,2048]{1,0:T(8,128)(2,1)S(1)}, bf16[96,2048]{1,0:T(8,128)(2,1)S(1)}, u32[]{:S(2)}, u32[]{:S(2)}) collective-permute-start(bf16[96,2048]{1,0:T(8,128)(2,1)S(1)} %get-tuple-element.20), channel_id=1, source_target_pairs={{0,3},{1,0},{2,1},{3,2},{4,7},{5,4},{6,5},{7,6},{8,11},{9,8},{10,9... | collective-permute-start | bytes 1179656 | tf_op jit(solution)/shard_map/ppermute | solution.py:271
  100.2 17.7 %collective-permute-start.16 = (bf16[96,2048]{1,0:T(8,128)(2,1)S(1)}, bf16[96,2048]{1,0:T(8,128)(2,1)S(1)}, u32[]{:S(2)}, u32[]{:S(2)}) collective-permute-start(bf16[96,2048]{1,0:T(8,128)(2,1)S(1)} %get-tuple-element.27), channel_id=1, source_target_pairs={{0,2},{1,3},{2,0},{3,1},{4,6},{5,7},{6,4},{7,5},{8,10},{9,11},{10,... | collective-permute-start | bytes 1179656 | tf_op jit(solution)/shard_map/ppermute | solution.py:271
  110.3 12.8 %collective-permute-start.15 = (bf16[96,2048]{1,0:T(8,128)(2,1)S(1)}, bf16[96,2048]{1,0:T(8,128)(2,1)}, u32[]{:S(2)}, u32[]{:S(2)}) collective-permute-start(bf16[96,2048]{1,0:T(8,128)(2,1)S(1)} %get-tuple-element.26), channel_id=1, source_target_pairs={{0,1},{1,2},{2,3},{3,0},{4,5},{5,6},{6,7},{7,4},{8,9},{9,10},{10,1... | collective-permute-start | bytes 1179656 | tf_op jit(solution)/shard_map/ppermute | solution.py:271
  111.5 11.7 %collective-permute-start.14 = (bf16[96,2048]{1,0:T(8,128)(2,1)S(1)}, bf16[96,2048]{1,0:T(8,128)(2,1)}, u32[]{:S(2)}, u32[]{:S(2)}) collective-permute-start(bf16[96,2048]{1,0:T(8,128)(2,1)S(1)} %get-tuple-element.25), channel_id=1, source_target_pairs={{0,3},{1,0},{2,1},{3,2},{4,7},{5,4},{6,5},{7,6},{8,11},{9,8},{10,9... | collective-permute-start | bytes 1179656 | tf_op jit(solution)/shard_map/ppermute | solution.py:271
  117.9 16.8 %collective-permute-start.3 = (bf16[1536,128]{1,0:T(8,128)(2,1)}, bf16[1536,128]{1,0:T(8,128)(2,1)S(1)}, u32[]{:S(2)}, u32[]{:S(2)}) collective-permute-start(bf16[1536,128]{1,0:T(8,128)(2,1)} %constant_dynamic-update-slice_fusion.refs_0_), channel_id=1, source_target_pairs={{0,16},{8,24},{16,0},{24,8},{1,17},{9,25},{17,1},{25,9},{2,18},{10... | collective-permute-start | bytes 1179656 | tf_op jit(solution)/shard_map/ppermute | solution.py:271
  125.6 30.5 %all-to-all-start.2 = ((bf16[32,96,128]{2,1,0:T(8,128)(2,1)}), bf16[32,96,128]{2,1,0:T(8,128)(2,1)S(1)}, u32[]{:S(2)}, u32[]{:S(2)}) async-start(bf16[32,96,128]{2,1,0:T(8,128)(2,1)} %pad_maximum_fusion), calls=%async_computation.3 | async-start | bytes 1572864 | tf_op jit(solution)/shard_map/all_to_all | solution.py:376
  134.3 52.0 %reduce-scatter.2.cloned.1.call-start = ((), (), s32[]{:S(2)}) async-start(), calls=%async_computation.5 | async-start | bytes 1216512 | tf_op jit(solution)/shard_map/reduce_scatter | solution.py:430
  134.7 0.8 copy-start.7
  156.5 1.8 collective-permute-start.17
  156.6 29.7 %copy-start.2 = (f32[128]{0:T(128)S(1)}, f32[128]{0:T(128)}, u32[]{:S(2)}) copy-start(f32[128]{0:T(128)} %param.26) | copy-start | bytes 1540
  186.3 0.9 copy-start.1
Sparse Core Ops, SparseCore 0:
  13.0 59.1 all-gather.1
  151.0 35.3 reduce-scatter.1
